TPU v7x, 32 devices: a whole 2x2x4 slice. The times are simulated.
32 devices in a mesh: ep: 4 (over y, x), tp: 8 (over z, core).
Axes of the slice: x: 2, y: 2, z: 4, core: 2. Of those that a mesh axis runs over, the one named last changes fastest.
Arguments:
- queries: bfloat16 [2048, 16, 128], P('ep', 'tp'), may hold values from -125 to 125
- keys: bfloat16 [2048, 16, 128], P('ep', 'tp'), may hold values from -9 to 9
- values: bfloat16 [2048, 16, 128], P('ep', 'tp'), may hold values from -6 to 6
- mixing: float32 [16], P('tp'), may hold values from 0.3 to 0.8
- head_gain: float32 [128], replicated, may hold values from 0.1 to 1.9
- out_weight: bfloat16 [16, 128, 2048], P('tp'), may hold values from -0.125 to 0.125
- tokens_b: bfloat16 [4096, 2048], P(('ep', 'tp')), may hold values from -6 to 6
- norm_gain: float32 [2048], replicated, may hold values from 0.1 to 1.9
- expert_ids: int32 [4096, 2], P(('ep', 'tp')), may hold values from 0 to 3, all different within a row; in each aligned block of 128 rows (0 to 127, 128 to 255, ...) at most 96 rows name the same one
- group_gate: float32 [4096], P(('ep', 'tp')), may hold values from 0.2 to 1
- expert_gate: float32 [4096, 2], P(('ep', 'tp')), may hold values from 0.1 to 0.9
- gate_weight: bfloat16 [4, 2048, 1024], P('ep', None, 'tp'), may hold values from -0.125 to 0.125
- up_weight: bfloat16 [4, 2048, 1024], P('ep', None, 'tp'), may hold values from -0.125 to 0.125
- down_weight: bfloat16 [4, 2048, 1024], P('ep', None, 'tp'), may hold values from -0.1875 to 0.1875
Outputs:
- mixed: bfloat16 [2048, 2048], P(('ep', 'tp'))
- routed: bfloat16 [4096, 2048], P(('ep', 'tp'))
Inputs may be any that keep to these rules, and one draw needn't show every extreme that they name: `expert_ids`: within each aligned block of 128 rows, no expert is named by more than 96 rows, and some block has an expert named by exactly 96 rows.
All inputs are finite; a program needn't handle non-finite values.
Results may differ from a plain program's by a relative error of at most 0.019.
Values may be sent and summed in bfloat16 or wider, within the bound.
A program may use at most 192 MiB of HBM per device.

v0:
```python
import math
import jax
import jax.numpy as jnp
from jax import lax
from jax.sharding import PartitionSpec as P

HEAD = 64


def attend_heads(queries, keys, values, mixing, head_gain):
    shard_rows = queries.shape[0]
    head_count = queries.shape[1]
    value_width = values.shape[2]
    query_start = lax.axis_index("ep") * shard_rows
    score_scale = 1.0 / math.sqrt(HEAD)
    query_pos = query_start + lax.iota(jnp.int32, shard_rows)

    def update(running, key_block, value_block, block_start):
        key_pos = block_start + lax.iota(jnp.int32, shard_rows)
        allowed = key_pos[None, :] <= query_pos[:, None]
        fresh = []
        for map_index in range(2):
            maximum, row_sum, numerator = running[3 * map_index : 3 * map_index + 3]
            offset = map_index * HEAD
            scores = (
                jnp.einsum(
                    "qhd,khd->hqk",
                    queries[:, :, offset : offset + HEAD],
                    key_block[:, :, offset : offset + HEAD],
                    preferred_element_type=jnp.float32,
                )
                * score_scale
            )
            scores = jnp.where(allowed[None], scores, -1e30)
            newmax = jnp.maximum(maximum, jnp.max(scores, axis=2))
            shrink = jnp.exp(maximum - newmax)
            weights = jnp.exp(scores - newmax[:, :, None])
            row_sum = row_sum * shrink + jnp.sum(weights, axis=2)
            numerator = numerator * shrink[:, :, None] + jnp.einsum(
                "hqk,khe->hqe",
                weights.astype(jnp.bfloat16),
                value_block,
                preferred_element_type=jnp.float32,
            )
            fresh += [newmax, row_sum, numerator]
        return tuple(fresh)

    floor_max = jnp.full((head_count, shard_rows), -1e30, jnp.float32)
    zero_sum = jnp.zeros((head_count, shard_rows), jnp.float32)
    zero_acc = jnp.zeros((head_count, shard_rows, value_width), jnp.float32)
    start_state = (floor_max, zero_sum, zero_acc, floor_max, zero_sum, zero_acc)
    running = start_state
    key_piece = lax.all_gather(keys, "ep", axis=0, tiled=True)
    value_piece = lax.all_gather(values, "ep", axis=0, tiled=True)
    blocks = key_piece.shape[0] // shard_rows
    key_blocks = key_piece.reshape(blocks, shard_rows, head_count, key_piece.shape[2])
    value_blocks = value_piece.reshape(blocks, shard_rows, head_count, value_width)

    def visit_block(state, inputs):
        key_block, value_block, block_index = inputs
        block_start = block_index * shard_rows
        state = lax.cond(
            block_start <= query_start + shard_rows - 1,
            lambda state_in: update(state_in, key_block, value_block, block_start),
            lambda state_in: state_in,
            state,
        )
        return (state, None)

    running, unused = lax.scan(
        visit_block, running, (key_blocks, value_blocks, lax.iota(jnp.int32, blocks))
    )
    state = running
    diff = state[2] / state[1][:, :, None] - mixing[:, None, None] * state[5] / state[4][:, :, None]
    normed = diff * lax.rsqrt(jnp.mean(diff * diff, axis=2, keepdims=True) + 1e-05) * head_gain
    return normed.astype(jnp.bfloat16)


def mixer_half(queries, keys, values, mixing, head_gain, out_weight):
    attended = attend_heads(queries, keys, values, mixing, head_gain)
    return lax.psum_scatter(
        jnp.einsum("hqe,hed->qd", attended, out_weight, preferred_element_type=jnp.float32).astype(
            jnp.bfloat16
        ),
        "tp",
        scatter_dimension=0,
        tiled=True,
    )


def expert_half(
    tokens_b, norm_gain, expert_ids, group_gate, expert_gate, gate_weight, up_weight, down_weight
):
    local_rows = tokens_b.shape[0]
    width = tokens_b.shape[1]
    top_count = expert_ids.shape[1]
    ep_count = lax.axis_size("ep")
    local_count = gate_weight.shape[0]
    expert_total = ep_count * local_count
    capacity = 3 * local_rows * top_count // (2 * expert_total)
    tokens_f = tokens_b.astype(jnp.float32)
    normed = (
        tokens_f
        * lax.rsqrt(jnp.mean(tokens_f * tokens_f, axis=1, keepdims=True) + 1e-06)
        * norm_gain
    ).astype(jnp.bfloat16)
    flat_ids = expert_ids.reshape(-1)
    one_hot = (flat_ids[:, None] == lax.iota(jnp.int32, expert_total)[None, :]).astype(jnp.int32)
    slot_rank = jnp.sum((jnp.cumsum(one_hot, axis=0) - one_hot) * one_hot, axis=1)
    slot_index = flat_ids * capacity + slot_rank
    owners = jnp.full((expert_total * capacity,), local_rows, jnp.int32)
    owners = owners.at[slot_index].set(lax.iota(jnp.int32, local_rows * top_count) // top_count)
    padded = jnp.concatenate([normed, jnp.zeros((1, width), jnp.bfloat16)], axis=0)
    outgoing = padded[owners].reshape(ep_count, local_count * capacity, width)
    incoming = lax.all_to_all(outgoing, "ep", split_axis=0, concat_axis=0, tiled=True)
    expert_rows = jnp.transpose(
        incoming.reshape(ep_count, local_count, capacity, width), (1, 0, 2, 3)
    )
    expert_rows = expert_rows.reshape(local_count, ep_count * capacity, width)
    piece_gate = lax.all_gather(gate_weight, "tp", axis=2, tiled=True)
    piece_up = lax.all_gather(up_weight, "tp", axis=2, tiled=True)
    piece_down = lax.all_gather(down_weight, "tp", axis=2, tiled=True)
    gate_part = jnp.einsum(
        "jrd,jdf->jrf", expert_rows, piece_gate, preferred_element_type=jnp.float32
    )
    up_part = jnp.einsum("jrd,jdf->jrf", expert_rows, piece_up, preferred_element_type=jnp.float32)
    hidden = (jax.nn.silu(gate_part) * up_part).astype(jnp.bfloat16)
    expert_out = jnp.einsum(
        "jrf,jdf->jrd", hidden, piece_down, preferred_element_type=jnp.float32
    ).astype(jnp.bfloat16)
    outbound = jnp.transpose(
        expert_out.reshape(local_count, ep_count, capacity, width), (1, 0, 2, 3)
    )
    outbound = outbound.reshape(ep_count, local_count * capacity, width)
    returned = lax.all_to_all(outbound, "ep", split_axis=0, concat_axis=0, tiled=True).reshape(
        expert_total * capacity, width
    )
    picked = returned[slot_index].reshape(local_rows, top_count, width).astype(jnp.float32)
    route_weight = group_gate[:, None] * expert_gate
    return jnp.sum(route_weight[:, :, None] * picked, axis=1).astype(jnp.bfloat16)


def per_device(
    queries,
    keys,
    values,
    mixing,
    head_gain,
    out_weight,
    tokens_b,
    norm_gain,
    expert_ids,
    group_gate,
    expert_gate,
    gate_weight,
    up_weight,
    down_weight,
):
    mixed = mixer_half(queries, keys, values, mixing, head_gain, out_weight)
    routed = expert_half(
        tokens_b,
        norm_gain,
        expert_ids,
        group_gate,
        expert_gate,
        gate_weight,
        up_weight,
        down_weight,
    )
    return (mixed, routed)


def solution(mesh):
    placed = (
        P("ep", "tp", None),
        P("ep", "tp", None),
        P("ep", "tp", None),
        P("tp"),
        P(),
        P("tp", None, None),
        P(("ep", "tp"), None),
        P(),
        P(("ep", "tp"), None),
        P(("ep", "tp")),
        P(("ep", "tp"), None),
        P("ep", None, "tp"),
        P("ep", None, "tp"),
        P("ep", None, "tp"),
    )
    return jax.shard_map(
        per_device,
        mesh=mesh,
        in_specs=placed,
        out_specs=(P(("ep", "tp"), None), P(("ep", "tp"), None)),
        check_vma=False,
    )
```

profile of v0, /device:TPU:0, one launch (start us, length us, event | category | flops | bytes accessed | tf_op | source)
XLA Modules:
  0.0 260.2 jit_solution(6079203360803837472)
XLA Ops:
  7.3 1.8 copy.24
  9.1 1.7 copy.25
  13.4 1.2 reduce-window.6
  15.3 1.4 scatter_custom_fusion
  17.0 1.0 fusion.33
  17.9 21.8 %all-gather.6.cloned.1.call-done = bf16[2048,2,128]{2,0,1:T(8,128)(2,1)} async-done(((bf16[512,2,128]{2,0,1:T(8,128)(2,1)}), bf16[2048,2,128]{2,0,1:T(8,128)(2,1)}) %all-gather.6.cloned.1.call-update) | async-done | bytes 1048592 | tf_op jit(solution)/shard_map/all_gather | solution.py:53
  39.7 2.3 copy.26
  42.0 26.1 %all-gather.8.cloned.1.call-done = bf16[2048,2,128]{2,0,1:T(8,128)(2,1)} async-done(((bf16[512,2,128]{2,0,1:T(8,128)(2,1)}), bf16[2048,2,128]{2,0,1:T(8,128)(2,1)}) %all-gather.8.cloned.1.call-update) | async-done | bytes 1048592 | tf_op jit(solution)/shard_map/all_gather | solution.py:54
  68.1 1.3 copy.28
  69.5 9.8 %while.23 = (s32[]{:T(128)}, f32[2,512]{1,0:T(2,128)S(1)}, f32[2,512]{1,0:T(2,128)S(1)}, f32[2,512,128]{2,1,0:T(8,128)S(1)}, f32[2,512]{1,0:T(2,128)S(1)}, /*ind...) while((s32[]{:T(128)}, f32[2,512]{1,0:T(2,128)S(1)}, ...), condition=%wide.region_7.8_spmd.clone, body=%wide.region_0.7_spmd.clone.sunk | while | flops 410784768 | bytes 17183128 | solution.py:70
  70.8 4.6 %conditional.3 = ((f32[2,512]{1,0:T(2,128)S(1)}, f32[2,512]{1,0:T(2,128)S(1)}, f32[2,512,128]{2,1,0:T(8,128)S(1)}, f32[2,512]{1,0:T(2,128)S(1)}, f32[2,512]{1,0:T(2,128)S(1)}, /*index=5*/f32[2,512,128]{2,1,0:T(8,128)S(1)})) conditional(s32[]{:T(128)} %convert_element_type.87, (f32[2,512]{1,0:T(2,128)S(1)}, f32[2,512]{1,0:T(2,128)S(1)}, ...), branch_computations={%region_1.1_spmd, %region_2.6_spmd} | conditional | flops 410784768 | bytes 17180748 | solution.py:62
  70.8 1.0 dynamic-slice_bitcast_fusion
  79.9 2.1 bitcast_convert_fusion
  82.2 2.5 gather_fusion
  84.6 36.1 %all_to_all.10 = bf16[4,96,2048]{2,1,0:T(8,128)(2,1)} all-to-all(bf16[4,96,2048]{2,1,0:T(8,128)(2,1)S(1)} %bitcast.62), channel_id=1, replica_groups=mesh['ep'=4,'tp'=8] {'ep'}, dimensions={0} | all-to-all | bytes 3145728 | tf_op jit(solution)/shard_map/all_to_all | solution.py:115
  120.7 5.7 %fusion.24 = f32[384,1024]{1,0:T(8,128)} fusion(bf16[384,2048]{1,0:T(8,128)(2,1)} %bitcast.63, bf16[1,2048,1024]{2,1,0:T(8,128)(2,1)} %all-gather.10.cloned.1.call-done), kind=kOutput, calls=%fused_computation.38 | convolution fusion | flops 1610612736 | bytes 7340032 | tf_op jit(solution)/shard_map/jrd,jdf->jrf/dot_general | solution.py:123
  126.4 38.6 %all-gather.12.cloned.1.call-done = bf16[1,2048,1024]{2,1,0:T(8,128)(2,1)} async-done(((bf16[1,2048,128]{2,1,0:T(8,128)(2,1)}), bf16[1,2048,1024]{2,1,0:T(8,128)(2,1)}) %all-gather.12.cloned.1.call-update) | async-done | bytes 4194320 | tf_op jit(solution)/shard_map/all_gather | solution.py:121
  165.0 47.5 %all-gather.14.cloned.1.call-done = bf16[1,2048,1024]{2,1,0:T(8,128)(2,1)} async-done(((bf16[1,2048,128]{2,1,0:T(8,128)(2,1)}), bf16[1,2048,1024]{2,1,0:T(8,128)(2,1)}) %all-gather.14.cloned.1.call-update) | async-done | bytes 4194320 | tf_op jit(solution)/shard_map/all_gather | solution.py:122
  212.5 8.6 %fusion.26 = bf16[384,2048]{1,0:T(8,128)(2,1)} fusion(bf16[1,2048,1024]{2,1,0:T(8,128)(2,1)} %all-gather.14.cloned.1.call-done, f32[384,1024]{1,0:T(8,128)} %fusion.24, bf16[384,2048]{1,0:T(8,128)(2,1)S(1)} %bitcast.64, bf16[1,2048,1024]{2,1,0:T(8,128)(2,1)} %all-gather.12.cloned.1.call-done), kind=kOutput, calls=%fused_computation.41 | convolution fusion | flops 3224371200 | bytes 13107200 | tf_op jit(solution)/shard_map/jrf,jdf->jrd/dot_general | solution.py:128
  221.1 3.8 %all-to-all-start.1 = ((bf16[4,96,2048]{2,1,0:T(8,128)(2,1)}), bf16[4,96,2048]{2,1,0:T(8,128)(2,1)S(1)}, u32[]{:S(2)}, u32[]{:S(2)}) async-start(bf16[4,96,2048]{2,1,0:T(8,128)(2,1)} %bitcast.65), calls=%async_computation.2 | async-start | bytes 3145728 | tf_op jit(solution)/shard_map/all_to_all | solution.py:135
  225.0 19.7 %all-to-all-done.1 = bf16[4,96,2048]{2,1,0:T(8,128)(2,1)S(1)} async-done(((bf16[4,96,2048]{2,1,0:T(8,128)(2,1)}), bf16[4,96,2048]{2,1,0:T(8,128)(2,1)S(1)}, u32[]{:S(2)}, u32[]{:S(2)}) %all-to-all-start.1) | async-done | bytes 1572896 | tf_op jit(solution)/shard_map/all_to_all | solution.py:135
  244.7 2.3 gather_fusion.1
  247.1 2.4 reshape.163
  249.4 3.9 %multiply_reduce_fusion = bf16[128,2048]{1,0:T(8,128)(2,1)} fusion(f32[128,2,2048]{2,1,0:T(2,128)S(1)} %reshape.163, f32[128,2]{1,0:T(8,128)S(1)} %copy.29), kind=kLoop, calls=%fused_computation.42 | loop fusion | flops 786432 | bytes 2622464 | tf_op jit(solution)/shard_map/reduce_sum | solution.py:140
  (95 shorter events, 10.3 us)
Async XLA Ops:
  7.2 72.7 %copy-start = (bf16[2,128,2048]{2,1,0:T(8,128)(2,1)S(1)}, bf16[2,128,2048]{2,1,0:T(8,128)(2,1)}, u32[]{:S(2)}) copy-start(bf16[2,128,2048]{2,1,0:T(8,128)(2,1)} %param.23) | copy-start | bytes 3145732
  7.2 5.6 %copy-start.6 = (s32[128,2]{0,1:T(2,128)S(1)}, s32[128,2]{0,1:T(2,128)}, u32[]{:S(2)}) copy-start(s32[128,2]{0,1:T(2,128)} %param.26) | copy-start | bytes 3076
  7.2 6.0 %copy-start.4 = (bf16[512,2,128]{2,1,0:T(2,128)(2,1)S(1)}, bf16[512,2,128]{2,1,0:T(2,128)(2,1)}, u32[]{:S(2)}) copy-start(bf16[512,2,128]{2,1,0:T(2,128)(2,1)} %param.18) | copy-start | bytes 786436
  7.2 9.5 %copy-start.1 = (bf16[128,2048]{1,0:T(8,128)(2,1)S(1)}, bf16[128,2048]{1,0:T(8,128)(2,1)}, u32[]{:S(2)}) copy-start(bf16[128,2048]{1,0:T(8,128)(2,1)} %param.24) | copy-start | bytes 1572868
  7.2 32.5 %all-gather.6.cloned.1.call-start = ((), (), s32[]{:S(2)}) async-start(), calls=%async_computation.3 | async-start | bytes 1310720 | tf_op jit(solution)/shard_map/all_gather | solution.py:53
  9.1 7.9 %copy-start.5 = (f32[2048]{0:T(1024)S(1)}, f32[2048]{0:T(1024)}, u32[]{:S(2)}) copy-start(f32[2048]{0:T(1024)} %param.25) | copy-start | bytes 24580
  9.1 59.0 %all-gather.8.cloned.1.call-start = ((), (), s32[]{:S(2)}) async-start(), calls=%async_computation.4 | async-start | bytes 1310720 | tf_op jit(solution)/shard_map/all_gather | solution.py:54
  10.8 109.8 %all-gather.10.cloned.1.call-start = ((), (), s32[]{:S(2)}) async-start(), calls=%async_computation.6 | async-start | bytes 4718592 | tf_op jit(solution)/shard_map/all_gather | solution.py:120
  11.6 153.4 %all-gather.12.cloned.1.call-start = ((), (), s32[]{:S(2)}) async-start(), calls=%async_computation.7 | async-start | bytes 4718592 | tf_op jit(solution)/shard_map/all_gather | solution.py:121
  12.2 200.3 %all-gather.14.cloned.1.call-start = ((), (), s32[]{:S(2)}) async-start(), calls=%async_computation.8 | async-start | bytes 4718592 | tf_op jit(solution)/shard_map/all_gather | solution.py:122
  12.7 240.6 %reduce-scatter.2.cloned.1.call-start = ((), (), s32[]{:S(2)}) async-start(), calls=%async_computation.5 | async-start | bytes 2359296 | tf_op jit(solution)/shard_map/reduce_scatter | solution.py:81
  69.5 9.9 %copy-start.8 = (f32[2]{0:T(128)S(1)}, f32[2]{0:T(128)}, u32[]{:S(2)}) copy-start(f32[2]{0:T(128)} %param.21) | copy-start | bytes 28
  69.5 10.4 %copy-start.9 = (f32[128]{0:T(128)S(1)}, f32[128]{0:T(128)}, u32[]{:S(2)}) copy-start(f32[128]{0:T(128)} %param.22) | copy-start | bytes 1540
  79.9 2.2 copy-start.2
  120.7 91.8 %copy-start.3 = (bf16[4,96,2048]{2,1,0:T(8,128)(2,1)S(1)}, bf16[4,96,2048]{2,1,0:T(8,128)(2,1)}, u32[]{:S(2)}) copy-start(bf16[4,96,2048]{2,1,0:T(8,128)(2,1)} %all_to_all.10) | copy-start | bytes 4718596
  221.1 3.8 %copy-start.7 = (f32[128,2]{0,1:T(2,128)S(1)}, f32[128,2]{0,1:T(2,128)}, u32[]{:S(2)}) copy-start(f32[128,2]{0,1:T(2,128)} %param.28) | copy-start | bytes 3076
  221.1 3.8 %copy-start.10 = (f32[128]{0:T(128)S(1)}, f32[128]{0:T(128)}, u32[]{:S(2)}) copy-start(f32[128]{0:T(128)} %param.27) | copy-start | bytes 1540
  221.1 23.6 %all-to-all-start.1 = ((bf16[4,96,2048]{2,1,0:T(8,128)(2,1)}), bf16[4,96,2048]{2,1,0:T(8,128)(2,1)S(1)}, u32[]{:S(2)}, u32[]{:S(2)}) async-start(bf16[4,96,2048]{2,1,0:T(8,128)(2,1)} %bitcast.65), calls=%async_computation.2 | async-start | bytes 3145728 | tf_op jit(solution)/shard_map/all_to_all | solution.py:135
Sparse Core Ops, SparseCore 0:
  10.4 29.2 all-gather.5
  41.5 26.4 all-gather.7
  69.7 47.8 all-gather.9
  119.0 45.9 all-gather.11
  166.4 45.9 all-gather.13
  215.2 34.1 reduce-scatter.1
where the time goes:
time: 261 us; the launch traced here: 260 us
  waiting for transfers between devices  155 us (59%)
  blocking collectives  36.1 us (14%)
  local copies, waits for them, and re-layouts  20.4 us (8%)
  matrix products  19.2 us (7%)
  between operations  14.4 us (6%)
  other arithmetic  7.89 us (3%)
  starting transfers between devices  4.02 us (2%)
  loops' own time  2.93 us (1%)
    all_gather x1, waiting for transfers between devices, expert_half(): piece_down = lax.all_gather(down_weight, 'tp', axis=2, tiled=True)  47.5 us
    all_gather x1, waiting for transfers between devices, expert_half(): piece_up = lax.all_gather(up_weight, 'tp', axis=2, tiled=True)  38.6 us
    all_to_all x1, blocking collectives, expert_half(): lax.all_to_all(outgoing, 'ep', split_axis=0, concat_axis=0, tiled=True)  36.1 us
    all_gather x1, waiting for transfers between devices, attend_heads(): value_piece = lax.all_gather(values, 'ep', axis=0, tiled=True)  26.1 us
    all_gather x1, waiting for transfers between devices, attend_heads(): key_piece = lax.all_gather(keys, 'ep', axis=0, tiled=True)  21.8 us
    all_to_all x1, waiting for transfers between devices, expert_half(): lax.all_to_all(outbound, 'ep', split_axis=0, concat_axis=0, tiled=True)  19.7 us
    dot_general x1, matrix products, expert_half(): jnp.einsum('jrf,jdf->jrd', hidden, piece_down, preferred_element_type=jnp...  8.63 us
    unnamed x28, local copies, waits for them, and re-layouts  7.42 us
  transfers between devices with their start and end apart: 7, of which 5 were waited for; matrix products, arithmetic and copies ran while one was open for 18% of the time, Pallas kernels for 0%

commit v1 on v0

--- a/solution.py
+++ b/solution.py
@@ -3,6 +3,7 @@
 import jax.numpy as jnp
 from jax import lax
 from jax.sharding import PartitionSpec as P
+from jax.lax import axis_index, axis_size, ppermute
 
 HEAD = 64
 
@@ -50,7 +51,16 @@
     zero_acc = jnp.zeros((head_count, shard_rows, value_width), jnp.float32)
     start_state = (floor_max, zero_sum, zero_acc, floor_max, zero_sum, zero_acc)
     running = start_state
-    key_piece = lax.all_gather(keys, "ep", axis=0, tiled=True)
+    count_all = axis_size("ep")
+    v_next = keys
+    frames = [v_next]
+    ready = sorted(((k, (k + 1) % count_all) for k in range(count_all)))
+    for d in range(1, count_all):
+        v_next = ppermute(v_next, "ep", ready)
+        frames.insert(0, v_next)
+    u_next = jnp.concatenate(frames, axis=0)
+    wide_out = axis_index("ep") + 1
+    key_piece = jnp.roll(u_next, wide_out * keys.shape[0], axis=0)
     value_piece = lax.all_gather(values, "ep", axis=0, tiled=True)
     blocks = key_piece.shape[0] // shard_rows
     key_blocks = key_piece.reshape(blocks, shard_rows, head_count, key_piece.shape[2])

time: 261 us -> 239 us (0.916)
  waiting for transfers between devices: 155 us -> 135 us
  starting transfers between devices: 4.02 us -> 7.78 us
  blocking collectives: 36.1 us -> 33 us
    ppermute x0 -> x3, waiting for transfers between devices: none -> 26.6 us  [attend_heads(): v_next = ppermute(v_next, 'ep', ready)]
    all_gather x1, waiting for transfers between devices: 26.1 us -> 0.01 us  [attend_heads(): value_piece = lax.all_gather(values, 'ep', axis=0, tiled=True)]
    all_gather x1 -> x0, waiting for transfers between devices: 21.8 us -> none  [attend_heads(): key_piece = lax.all_gather(keys, 'ep', axis=0, tiled=True)]
    all_gather x1, waiting for transfers between devices: 38.6 us -> 47.5 us  [expert_half(): piece_up = lax.all_gather(up_weight, 'tp', axis=2, tiled=True)]
    all_gather x1, waiting for transfers between devices: 47.5 us -> 39.4 us  [expert_half(): piece_down = lax.all_gather(down_weight, 'tp', axis=2, tiled=True)]
    ppermute x0 -> x3, starting transfers between devices: none -> 3.81 us  [attend_heads(): v_next = ppermute(v_next, 'ep', ready)]
    all_to_all x1, blocking collectives: 36.1 us -> 33 us  [expert_half(): lax.all_to_all(outgoing, 'ep', split_axis=0, concat_axis=0, tiled=True)]
    unnamed x28 -> x37, local copies, waits for them, and re-layouts: 7.42 us -> 5.08 us
  transfers between devices with their start and end apart: 7 -> 9, of which waited for: 5 -> 6; matrix products, arithmetic and copies ran while one was open for 18% -> 18% of each run, Pallas kernels for 0% -> 0%
where the time goes in v1:
time: 239 us; the launch traced here: 238 us
  waiting for transfers between devices  135 us (56%)
  blocking collectives  33 us (14%)
  matrix products  19.2 us (8%)
  local copies, waits for them, and re-layouts  18.2 us (8%)
  between operations  14.1 us (6%)
  other arithmetic  7.89 us (3%)
  starting transfers between devices  7.78 us (3%)
  loops' own time  2.91 us (1%)
    all_gather x1, waiting for transfers between devices, expert_half(): piece_up = lax.all_gather(up_weight, 'tp', axis=2, tiled=True)  47.5 us
    all_gather x1, waiting for transfers between devices, expert_half(): piece_down = lax.all_gather(down_weight, 'tp', axis=2, tiled=True)  39.4 us
    all_to_all x1, blocking collectives, expert_half(): lax.all_to_all(outgoing, 'ep', split_axis=0, concat_axis=0, tiled=True)  33 us
    ppermute x3, waiting for transfers between devices, attend_heads(): v_next = ppermute(v_next, 'ep', ready)  26.6 us
    all_to_all x1, waiting for transfers between devices, expert_half(): lax.all_to_all(outbound, 'ep', split_axis=0, concat_axis=0, tiled=True)  19.7 us
    dot_general x1, matrix products, expert_half(): jnp.einsum('jrf,jdf->jrd', hidden, piece_down, preferred_element_type=jnp...  8.63 us
    dot_general x1, matrix products, expert_half(): jnp.einsum('jrd,jdf->jrf', expert_rows, piece_gate, preferred_element_typ...  5.74 us
    unnamed x37, local copies, waits for them, and re-layouts  5.08 us
  transfers between devices with their start and end apart: 9, of which 6 were waited for; matrix products, arithmetic and copies ran while one was open for 18% of the time, Pallas kernels for 0%

profile of v1, /device:TPU:0, one launch (start us, length us, event | category | flops | bytes accessed | tf_op | source)
XLA Modules:
  0.0 238.1 jit_solution(17905905904219754620)
XLA Ops:
  7.3 1.8 copy.27
  11.3 3.0 %collective-permute-start = (bf16[512,2,128]{2,0,1:T(8,128)(2,1)S(1)}, bf16[512,2,128]{2,0,1:T(8,128)(2,1)S(1)}, u32[]{:S(2)}, u32[]{:S(2)}) collective-permute-start(bf16[512,2,128]{2,0,1:T(8,128)(2,1)S(1)} %copy.24), channel_id=1, source_target_pairs={{0,8},{8,16},{16,24},{24,0},{1,9},{9,17},{17,25},{25,1},{2,10},{10... | collective-permute-start | bytes 786440 | tf_op jit(solution)/shard_map/ppermute | solution.py:59
  14.8 1.0 fusion.33
  15.9 1.2 reduce-window.6
  17.5 4.0 %collective-permute-done = bf16[512,2,128]{2,0,1:T(8,128)(2,1)S(1)} collective-permute-done((bf16[512,2,128]{2,0,1:T(8,128)(2,1)S(1)}, bf16[512,2,128]{2,0,1:T(8,128)(2,1)S(1)}, u32[]{:S(2)}, u32[]{:S(2)}) %collective-permute-start) | collective-permute-done | bytes 262176 | tf_op jit(solution)/shard_map/ppermute | solution.py:59
  22.6 10.0 %collective-permute-done.1 = bf16[512,2,128]{2,0,1:T(8,128)(2,1)S(1)} collective-permute-done((bf16[512,2,128]{2,0,1:T(8,128)(2,1)S(1)}, bf16[512,2,128]{2,0,1:T(8,128)(2,1)S(1)}, u32[]{:S(2)}, u32[]{:S(2)}) %collective-permute-start.1) | collective-permute-done | bytes 262176 | tf_op jit(solution)/shard_map/ppermute | solution.py:59
  32.8 1.4 scatter_custom_fusion
  34.2 12.6 %collective-permute-done.2 = bf16[512,2,128]{2,0,1:T(8,128)(2,1)S(1)} collective-permute-done((bf16[512,2,128]{2,0,1:T(8,128)(2,1)S(1)}, bf16[512,2,128]{2,0,1:T(8,128)(2,1)S(1)}, u32[]{:S(2)}, u32[]{:S(2)}) %collective-permute-start.2) | collective-permute-done | bytes 262176 | tf_op jit(solution)/shard_map/ppermute | solution.py:59
  47.2 1.3 copy.28
  48.6 1.3 copy.30
  50.1 9.8 %while.23 = (s32[]{:T(128)}, f32[2,512]{1,0:T(2,128)S(1)}, f32[2,512]{1,0:T(2,128)S(1)}, f32[2,512,128]{2,1,0:T(8,128)S(1)}, f32[2,512]{1,0:T(2,128)S(1)}, /*ind...) while((s32[]{:T(128)}, f32[2,512]{1,0:T(2,128)S(1)}, ...), condition=%wide.region_7.8_spmd.clone, body=%wide.region_0.7_spmd.clone.sunk | while | flops 410784768 | bytes 17183128 | solution.py:80
  51.3 4.6 %conditional.3 = ((f32[2,512]{1,0:T(2,128)S(1)}, f32[2,512]{1,0:T(2,128)S(1)}, f32[2,512,128]{2,1,0:T(8,128)S(1)}, f32[2,512]{1,0:T(2,128)S(1)}, f32[2,512]{1,0:T(2,128)S(1)}, /*index=5*/f32[2,512,128]{2,1,0:T(8,128)S(1)})) conditional(s32[]{:T(128)} %convert_element_type.87, (f32[2,512]{1,0:T(2,128)S(1)}, f32[2,512]{1,0:T(2,128)S(1)}, ...), branch_computations={%region_1.1_spmd, %region_2.6_spmd} | conditional | flops 410784768 | bytes 17180748 | solution.py:72
  60.4 2.1 bitcast_convert_fusion
  62.7 2.5 %gather_fusion = bf16[384,2048]{1,0:T(8,128)(2,1)S(1)} fusion(bf16[129,2048]{1,0:T(8,128)(2,1)S(1)} %concatenate.10, s32[1024]{0:T(1024)S(1)} %pad_clamp_fusion.1), kind=kCustom, calls=%fused_computation | custom fusion | bytes 3147264 | tf_op jit(solution)/shard_map/gather | solution.py:124
  65.1 33.0 %all_to_all.10 = bf16[4,96,2048]{2,1,0:T(8,128)(2,1)} all-to-all(bf16[4,96,2048]{2,1,0:T(8,128)(2,1)S(1)} %bitcast.62), channel_id=1, replica_groups=mesh['ep'=4,'tp'=8] {'ep'}, dimensions={0} | all-to-all | bytes 3145728 | tf_op jit(solution)/shard_map/all_to_all | solution.py:125
  98.1 5.7 %fusion.24 = f32[384,1024]{1,0:T(8,128)} fusion(bf16[384,2048]{1,0:T(8,128)(2,1)} %bitcast.64, bf16[1,2048,1024]{2,1,0:T(8,128)(2,1)} %all-gather.7.cloned.1.call-done), kind=kOutput, calls=%fused_computation.38 | convolution fusion | flops 1610612736 | bytes 7340032 | tf_op jit(solution)/shard_map/jrd,jdf->jrf/dot_general | solution.py:133
  103.8 39.4 %all-gather.11.cloned.1.call-done = bf16[1,2048,1024]{2,1,0:T(8,128)(2,1)} async-done(((bf16[1,2048,128]{2,1,0:T(8,128)(2,1)}), bf16[1,2048,1024]{2,1,0:T(8,128)(2,1)}) %all-gather.11.cloned.1.call-update) | async-done | bytes 4194320 | tf_op jit(solution)/shard_map/all_gather | solution.py:132
  143.2 47.5 %all-gather.9.cloned.1.call-done = bf16[1,2048,1024]{2,1,0:T(8,128)(2,1)} async-done(((bf16[1,2048,128]{2,1,0:T(8,128)(2,1)}), bf16[1,2048,1024]{2,1,0:T(8,128)(2,1)}) %all-gather.9.cloned.1.call-update) | async-done | bytes 4194320 | tf_op jit(solution)/shard_map/all_gather | solution.py:131
  190.7 8.6 %fusion.26 = bf16[384,2048]{1,0:T(8,128)(2,1)} fusion(bf16[1,2048,1024]{2,1,0:T(8,128)(2,1)} %all-gather.11.cloned.1.call-done, f32[384,1024]{1,0:T(8,128)} %fusion.24, bf16[384,2048]{1,0:T(8,128)(2,1)S(1)} %bitcast.65, bf16[1,2048,1024]{2,1,0:T(8,128)(2,1)} %all-gather.9.cloned.1.call-done), kind=kOutput, calls=%fused_computation.41 | convolution fusion | flops 3224371200 | bytes 13107200 | tf_op jit(solution)/shard_map/jrf,jdf->jrd/dot_general | solution.py:138
  199.3 3.8 %all-to-all-start.1 = ((bf16[4,96,2048]{2,1,0:T(8,128)(2,1)}), bf16[4,96,2048]{2,1,0:T(8,128)(2,1)S(1)}, u32[]{:S(2)}, u32[]{:S(2)}) async-start(bf16[4,96,2048]{2,1,0:T(8,128)(2,1)} %bitcast.66), calls=%async_computation.2 | async-start | bytes 3145728 | tf_op jit(solution)/shard_map/all_to_all | solution.py:145
  203.2 19.7 %all-to-all-done.1 = bf16[4,96,2048]{2,1,0:T(8,128)(2,1)S(1)} async-done(((bf16[4,96,2048]{2,1,0:T(8,128)(2,1)}), bf16[4,96,2048]{2,1,0:T(8,128)(2,1)S(1)}, u32[]{:S(2)}, u32[]{:S(2)}) %all-to-all-start.1) | async-done | bytes 1572896 | tf_op jit(solution)/shard_map/all_to_all | solution.py:145
  222.9 2.3 gather_fusion.1
  225.3 2.4 reshape.163
  227.7 3.9 %multiply_reduce_fusion = bf16[128,2048]{1,0:T(8,128)(2,1)} fusion(f32[128,2,2048]{2,1,0:T(2,128)S(1)} %reshape.163, f32[128,2]{1,0:T(8,128)S(1)} %copy.31), kind=kLoop, calls=%fused_computation.42 | loop fusion | flops 786432 | bytes 2622464 | tf_op jit(solution)/shard_map/reduce_sum | solution.py:150
  (109 shorter events, 12.6 us)
Async XLA Ops:
  7.2 53.2 %copy-start = (bf16[2,128,2048]{2,1,0:T(8,128)(2,1)S(1)}, bf16[2,128,2048]{2,1,0:T(8,128)(2,1)}, u32[]{:S(2)}) copy-start(bf16[2,128,2048]{2,1,0:T(8,128)(2,1)} %param.23) | copy-start | bytes 3145732
  7.2 4.0 %copy-start.1 = (bf16[512,2,128]{2,1,0:T(2,128)(2,1)S(1)}, bf16[512,2,128]{2,1,0:T(2,128)(2,1)}, u32[]{:S(2)}) copy-start(bf16[512,2,128]{2,1,0:T(2,128)(2,1)} %param.19) | copy-start | bytes 786436
  7.2 7.1 %copy-start.7 = (s32[128,2]{0,1:T(2,128)S(1)}, s32[128,2]{0,1:T(2,128)}, u32[]{:S(2)}) copy-start(s32[128,2]{0,1:T(2,128)} %param.26) | copy-start | bytes 3076
  7.2 7.4 %copy-start.2 = (bf16[128,2048]{1,0:T(8,128)(2,1)S(1)}, bf16[128,2048]{1,0:T(8,128)(2,1)}, u32[]{:S(2)}) copy-start(bf16[128,2048]{1,0:T(8,128)(2,1)} %param.24) | copy-start | bytes 1572868
  7.2 7.6 %copy-start.6 = (f32[2048]{0:T(1024)S(1)}, f32[2048]{0:T(1024)}, u32[]{:S(2)}) copy-start(f32[2048]{0:T(1024)} %param.25) | copy-start | bytes 24580
  7.2 41.4 %all-gather.5.cloned.1.call-start = ((), (), s32[]{:S(2)}) async-start(), calls=%async_computation.3 | async-start | bytes 1310720 | tf_op jit(solution)/shard_map/all_gather | solution.py:64
  9.1 23.5 %copy-start.5 = (bf16[512,2,128]{2,1,0:T(2,128)(2,1)S(1)}, bf16[512,2,128]{2,1,0:T(2,128)(2,1)}, u32[]{:S(2)}) copy-start(bf16[512,2,128]{2,1,0:T(2,128)(2,1)} %param.18) | copy-start | bytes 786436
  9.1 89.0 %all-gather.7.cloned.1.call-start = ((), (), s32[]{:S(2)}) async-start(), calls=%async_computation.5 | async-start | bytes 4718592 | tf_op jit(solution)/shard_map/all_gather | solution.py:130
  9.9 133.3 %all-gather.11.cloned.1.call-start = ((), (), s32[]{:S(2)}) async-start(), calls=%async_computation.7 | async-start | bytes 4718592 | tf_op jit(solution)/shard_map/all_gather | solution.py:132
  10.6 180.1 %all-gather.9.cloned.1.call-start = ((), (), s32[]{:S(2)}) async-start(), calls=%async_computation.6 | async-start | bytes 4718592 | tf_op jit(solution)/shard_map/all_gather | solution.py:131
  11.2 220.4 %reduce-scatter.2.cloned.1.call-start = ((), (), s32[]{:S(2)}) async-start(), calls=%async_computation.4 | async-start | bytes 2359296 | tf_op jit(solution)/shard_map/reduce_scatter | solution.py:91
  11.3 10.3 %collective-permute-start = (bf16[512,2,128]{2,0,1:T(8,128)(2,1)S(1)}, bf16[512,2,128]{2,0,1:T(8,128)(2,1)S(1)}, u32[]{:S(2)}, u32[]{:S(2)}) collective-permute-start(bf16[512,2,128]{2,0,1:T(8,128)(2,1)S(1)} %copy.24), channel_id=1, source_target_pairs={{0,8},{8,16},{16,24},{24,0},{1,9},{9,17},{17,25},{25,1},{2,10},{10... | collective-permute-start | bytes 786440 | tf_op jit(solution)/shard_map/ppermute | solution.py:59
  21.6 11.0 %collective-permute-start.1 = (bf16[512,2,128]{2,0,1:T(8,128)(2,1)S(1)}, bf16[512,2,128]{2,0,1:T(8,128)(2,1)S(1)}, u32[]{:S(2)}, u32[]{:S(2)}) collective-permute-start(bf16[512,2,128]{2,0,1:T(8,128)(2,1)S(1)} %collective-permute-done), channel_id=1, source_target_pairs={{0,8},{8,16},{16,24},{24,0},{1,9},{9,17},{17,25},{25,1},{2,10},{10... | collective-permute-start | bytes 786440 | tf_op jit(solution)/shard_map/ppermute | solution.py:59
  32.6 14.2 %collective-permute-start.2 = (bf16[512,2,128]{2,0,1:T(8,128)(2,1)S(1)}, bf16[512,2,128]{2,0,1:T(8,128)(2,1)S(1)}, u32[]{:S(2)}, u32[]{:S(2)}) collective-permute-start(bf16[512,2,128]{2,0,1:T(8,128)(2,1)S(1)} %collective-permute-done.1), channel_id=1, source_target_pairs={{0,8},{8,16},{16,24},{24,0},{1,9},{9,17},{17,25},{25,1},{2,10},{10... | collective-permute-start | bytes 786440 | tf_op jit(solution)/shard_map/ppermute | solution.py:59
  50.0 9.8 %copy-start.9 = (f32[2]{0:T(128)S(1)}, f32[2]{0:T(128)}, u32[]{:S(2)}) copy-start(f32[2]{0:T(128)} %param.21) | copy-start | bytes 28
  50.0 10.4 %copy-start.10 = (f32[128]{0:T(128)S(1)}, f32[128]{0:T(128)}, u32[]{:S(2)}) copy-start(f32[128]{0:T(128)} %param.22) | copy-start | bytes 1540
  60.4 2.2 copy-start.3
  98.1 92.6 %copy-start.4 = (bf16[4,96,2048]{2,1,0:T(8,128)(2,1)S(1)}, bf16[4,96,2048]{2,1,0:T(8,128)(2,1)}, u32[]{:S(2)}) copy-start(bf16[4,96,2048]{2,1,0:T(8,128)(2,1)} %all_to_all.10) | copy-start | bytes 4718596
  199.3 3.8 %copy-start.8 = (f32[128,2]{0,1:T(2,128)S(1)}, f32[128,2]{0,1:T(2,128)}, u32[]{:S(2)}) copy-start(f32[128,2]{0,1:T(2,128)} %param.28) | copy-start | bytes 3076
  199.3 3.8 %copy-start.11 = (f32[128]{0:T(128)S(1)}, f32[128]{0:T(128)}, u32[]{:S(2)}) copy-start(f32[128]{0:T(128)} %param.27) | copy-start | bytes 1540
  199.3 23.6 %all-to-all-start.1 = ((bf16[4,96,2048]{2,1,0:T(8,128)(2,1)}), bf16[4,96,2048]{2,1,0:T(8,128)(2,1)S(1)}, u32[]{:S(2)}, u32[]{:S(2)}) async-start(bf16[4,96,2048]{2,1,0:T(8,128)(2,1)} %bitcast.66), calls=%async_computation.2 | async-start | bytes 3145728 | tf_op jit(solution)/shard_map/all_to_all | solution.py:145
Sparse Core Ops, SparseCore 0:
  10.4 36.5 all-gather.4
  48.7 46.8 all-gather.6
  97.2 45.9 all-gather.10
  144.7 45.9 all-gather.8
  193.4 33.9 reduce-scatter.1
